TPU v7x, 32 devices: a whole 2x2x4 slice. The times are simulated.
32 devices in a mesh: rep: 2 (over y), fs: 4 (over z), tp: 4 (over x, core).
Axes of the slice: x: 2, y: 2, z: 4, core: 2. Of those that a mesh axis runs over, the one named last changes fastest.
Arguments:
- tokens: bfloat16 [2048, 2048], P(('rep', 'fs')), may hold values from -6 to 6
- mix_gain: float32 [2048], replicated, may hold values from 0.1 to 1.9
- group_weight: float32 [512, 2048], P('fs', 'tp'), may hold values from -0.25 to 0.25
- group_scale: float32 [1, 2048], P(None, 'tp'), may hold values from 0.5 to 2
- mlp_gain: float32 [2048], replicated, may hold values from 0.1 to 1.9
- up_weight: float32 [2048, 8192], P('fs', 'tp'), may hold values from -0.125 to 0.125
- up_scale: float32 [1, 8192], P(None, 'tp'), may hold values from 0.5 to 2
- down_weight: float32 [8192, 2048], P('tp', 'fs'), may hold values from -0.0625 to 0.0625
- down_scale: float32 [1, 2048], replicated, may hold values from 0.5 to 2
Outputs:
- layer_out: bfloat16 [2048, 2048], P(('rep', 'fs'))
All inputs are finite; a program needn't handle non-finite values.
Results may differ from a plain program's by a relative error of at most 0.013.
Values may be sent and summed in bfloat16 or wider, within the bound.
A program may use at most 64 MiB of HBM per device.

v0:
```python
import functools

import jax
import jax.numpy as jnp
from jax import lax
from jax.experimental import pallas as pl
from jax.experimental.pallas import tpu as pltpu
from jax.sharding import PartitionSpec as P

GROUPS = 4
LENGTH = 128


norm_eps = 1e-06


def norm_rows(values, gain):
    promoted = values.astype(jnp.float32)
    inverse = lax.rsqrt(jnp.mean(promoted * promoted, axis=-1, keepdims=True) + norm_eps)
    return (promoted * inverse * gain).astype(jnp.bfloat16)


def band_means(inputs, window, seq_length):
    row_count, columns = inputs.shape
    by_sequence = inputs.reshape(row_count // seq_length, seq_length, columns)
    position = jnp.arange(seq_length, dtype=jnp.int32)
    offset = position[:, None] - position[None, :]
    band_mask = ((offset >= 0) & (offset < window)).astype(jnp.bfloat16)
    divisor = jnp.minimum(position + 1, window).astype(jnp.float32)
    summed = jnp.einsum("ts,nsc->ntc", band_mask, by_sequence, preferred_element_type=jnp.float32)
    return (summed / divisor[None, :, None] - by_sequence.astype(jnp.float32)).reshape(
        row_count, columns
    )


def body(
    tokens,
    mix_gain,
    group_weight,
    group_scale,
    mlp_gain,
    up_weight,
    up_scale,
    down_weight,
    down_scale,
):
    model_width = tokens.shape[1]
    group_width = model_width // GROUPS
    own_cols = group_weight.shape[1]
    column_start = lax.axis_index("tp") * own_cols
    group_index = column_start // group_width
    normed = norm_rows(tokens, mix_gain)
    inputs = lax.dynamic_slice_in_dim(normed, group_index * group_width, group_width, 1)
    window = jnp.left_shift(jnp.int32(2), group_index)
    pooled = band_means(inputs, window, LENGTH).astype(jnp.bfloat16)
    mixed_cols = (
        jnp.dot(
            pooled,
            lax.all_gather(group_weight.astype(jnp.bfloat16), "fs", axis=0, tiled=True),
            preferred_element_type=jnp.float32,
        )
        * group_scale
    )
    own_tokens = lax.dynamic_slice_in_dim(tokens, column_start, own_cols, 1)
    carried_cols = (own_tokens.astype(jnp.float32) + mixed_cols).astype(jnp.bfloat16)
    carried = lax.all_gather(carried_cols, "tp", axis=1, tiled=True)
    normed_mlp = norm_rows(carried, mlp_gain)
    pre_act = (
        jnp.dot(
            normed_mlp,
            lax.all_gather(up_weight.astype(jnp.bfloat16), "fs", axis=0, tiled=True),
            preferred_element_type=jnp.float32,
        )
        * up_scale
    )
    hidden = jnp.square(jax.nn.relu(pre_act)).astype(jnp.bfloat16)
    partial_value = (
        jnp.dot(
            hidden,
            lax.all_gather(down_weight.astype(jnp.bfloat16), "fs", axis=1, tiled=True),
            preferred_element_type=jnp.float32,
        )
        * down_scale
    )
    summed = lax.psum(partial_value.astype(jnp.bfloat16), "tp").astype(jnp.float32)
    return (carried.astype(jnp.float32) + summed).astype(jnp.bfloat16)


MESH = pl.DeviceIdType.MESH


def ring_kernel(
    sizes,
    tok_h, mg, gw_h, gs, lg, up_h, us, dn_h, ds,
    out_h,
    tok, gwf, upf, upo, dnf, dno,
    gwg, ups, upg, dns, dng,
    car, xn, hid, pb, ra, sx, rb, sz, rc, og,
    ld, sw, rw, sy, ry, scz, rcz, scx, rcx, scc, rcc,
    sa, ra_s, sb, rb_s, st, rt, so, ro, wr,
):
    Z, T, rows, D, own, hg, hu, hd, fsub, dsub = sizes
    r, z, t = lax.axis_index("rep"), lax.axis_index("fs"), lax.axis_index("tp")
    cp = t + 1 - 2 * lax.rem(t, 2)
    xp = lax.rem(t + 2, T)
    cxp = lax.rem(cp + 2, T)
    peer_r = 1 - r
    bf, f32 = jnp.bfloat16, jnp.float32

    def mul(i, n):
        return pl.multiple_of(i * n, n)

    def zat(d):
        return lax.rem(z + d, Z)

    loads = {}

    def load(key, src, dst, k):
        c = pltpu.make_async_copy(src, dst, ld.at[k])
        c.start()
        loads[key] = c

    load("gw", gw_h, gwf, 0)
    load("tok", tok_h, tok, 1)
    order = list(range(1, Z)) + [0]
    for d in order:
        zd = zat(d)
        load(("up", d), up_h.at[pl.ds(mul(r, hu), hu), pl.ds(mul(zd, fsub), fsub)], upf.at[d], 2 + d)
    for d in order:
        zd = zat(d)
        load(("dn", d), dn_h.at[pl.ds(pl.multiple_of(zd * 2 * hd + r * hd, hd), hd), :], dnf.at[d], 2 + Z + d)
    load("upo", up_h.at[pl.ds(mul(peer_r, hu), hu), pl.ds(mul(z, fsub), fsub)], upo, 2 + 2 * Z)
    load("dno", dn_h.at[pl.ds(pl.multiple_of(z * 2 * hd + peer_r * hd, hd), hd), :], dno, 3 + 2 * Z)

    barrier = pltpu.get_barrier_semaphore()
    peers = [(r, zat(d), t) for d in range(1, Z)] + [(peer_r, z, t), (r, z, xp), (r, z, cp)]
    for p in peers:
        pl.semaphore_signal(barrier, inc=1, device_id=p, device_id_type=MESH)
    loads["gw"].wait()
    gwg[pl.ds(mul(z, 2 * hg), 2 * hg), :] = gwf[...].astype(bf)
    pl.semaphore_wait(barrier, len(peers))

    sends = []

    def remote(src, dst, ss, rs, dev):
        return pltpu.make_async_remote_copy(
            src_ref=src, dst_ref=dst, send_sem=ss, recv_sem=rs, device_id=dev, device_id_type=MESH
        )

    def send(src, dst, ss, rs, dev, when=None):
        if when is None:
            remote(src, dst, ss, rs, dev).start()
        else:
            pl.when(when)(lambda: remote(src, dst, ss, rs, dev).start())
        sends.append((when, (src, dst, ss, rs, dev)))

    def drain():
        for when, args in sends:
            if when is None:
                remote(*args).wait_send()
            else:
                pl.when(when)(lambda args=args: remote(*args).wait_send())

    def got(dst, ss, rs):
        remote(dst, dst, ss, rs, (peer_r, z, t)).wait_recv()

    def gw_at(src, rep):
        return gwg.at[pl.ds(pl.multiple_of(src * 2 * hg + rep * hg, hg), hg), :]

    def up_at(src, rep):
        return upg.at[pl.ds(pl.multiple_of(src * 2 * hu + rep * hu, hu), hu), :]

    def dn_at(src, rep):
        return dng.at[src, pl.ds(mul(rep, hd), hd), :]

    place = (gw_at, up_at, dn_at)

    for d in range(1, Z):
        send(gw_at(z, r), gw_at(z, r), sw.at[0, d], rw.at[0, z], (r, zat(d), t))
    ready = []
    for w, key, raw, cast in ((1, "up", upf, ups), (2, "dn", dnf, dns)):
        for d in range(1, Z):
            loads[(key, d)].wait()
            cast[d] = raw[d].astype(bf)
            ready.append((cast.at[d], place[w](z, r), sw.at[w, d], rw.at[w, z], (r, zat(d), t)))
            if w == 1 and d > 1 or w == 2 and d == 1:
                send(*ready.pop(0))
    loads[("up", 0)].wait()
    upg[pl.ds(pl.multiple_of(z * 2 * hu + r * hu, hu), hu), :] = upf[0].astype(bf)
    loads["upo"].wait()
    upg[pl.ds(pl.multiple_of(z * 2 * hu + peer_r * hu, hu), hu), :] = upo[...].astype(bf)
    loads[("dn", 0)].wait()
    dng[z, pl.ds(mul(r, hd), hd), :] = dnf[0].astype(bf)
    loads["dno"].wait()
    dng[z, pl.ds(mul(peer_r, hd), hd), :] = dno[...].astype(bf)

    loads["tok"].wait()
    full = tok[...].astype(f32)
    inv = lax.rsqrt(jnp.mean(full * full, axis=-1, keepdims=True) + norm_eps)
    cols = pl.ds(mul(t, own), own)
    mine = tok[:, cols].astype(f32)
    normed = (mine * inv * mg[:, cols]).astype(bf)
    window = jnp.left_shift(jnp.int32(2), t)
    ti = lax.broadcasted_iota(jnp.int32, (LENGTH, LENGTH), 0)
    si = lax.broadcasted_iota(jnp.int32, (LENGTH, LENGTH), 1)
    band = jnp.where((ti - si >= 0) & (ti - si < window), 1.0, 0.0).astype(bf)
    pos = lax.broadcasted_iota(jnp.int32, (LENGTH, own), 0)
    divisor = jnp.minimum(pos + 1, window).astype(f32)
    pooled = []
    for s in range(rows // LENGTH):
        part = normed[s * LENGTH:(s + 1) * LENGTH]
        summed = jnp.dot(band, part, preferred_element_type=f32)
        pooled.append((summed / divisor - part.astype(f32)).astype(bf))
    pooled = jnp.concatenate(pooled, axis=0)

    def swap_one(w, d):
        src = zat(Z - d)
        got(place[w](src, r), sw.at[w, d], rw.at[w, src])
        send(place[w](src, r), place[w](src, r), sy.at[w, d], ry.at[w, src], (peer_r, z, t))

    def swap(w):
        for d in range(1, Z):
            swap_one(w, d)

    def swapped(w):
        for d in range(1, Z):
            src = zat(Z - d)
            got(place[w](src, peer_r), sy.at[w, d], ry.at[w, src])

    swap(0)
    swapped(0)
    mixed = jnp.dot(pooled, gwg[...], preferred_element_type=f32) * gs[...]
    car[z, t] = (mine + mixed).astype(bf)
    H = rows // LENGTH
    hr = LENGTH
    side = 1 - 2 * lax.div(z, Z // 2)

    inner = lax.div(Z - 1 - side * (Z - 1 - 2 * z), 2)

    def src_of(d):
        if d == 0:
            return z
        near = (d + 1) // 2 if d % 2 else -(d // 2)
        both_sides = lax.div(2 * inner - d + 2 * Z, 2 * Z)
        return z + side * (both_sides * near + (1 - both_sides) * (d - inner))

    def half(h):
        return pl.ds(h * hr, hr)

    def to_x(src, h):
        b = car.at[src, t, half(h)]
        send(b, b, scx.at[src, h], rcx.at[src, h], (r, z, xp))

    def to_core(src, h, q, k):
        b = car.at[src, q, half(h)]
        send(b, b, scc.at[src, k, h], rcc.at[src, k, h], (r, z, cp))

    def to_z(src, h, when_up, when_down):
        b = car.at[src, t, half(h)]
        send(b, b, scz.at[0, src, h], rcz.at[src, h], (r, lax.rem(z + 1, Z), t), when_up)
        send(b, b, scz.at[1, src, h], rcz.at[src, h], (r, lax.rem(z + Z - 1, Z), t), when_down)

    for h in range(H):
        to_z(z, h, z < Z - 1, z > 0)
        to_x(z, h)
        to_core(z, h, t, 0)
    for args in ready:
        send(*args)

    def arrive(d, h):
        src = src_of(d)
        got(car.at[src, t, half(h)], scz.at[0, src, h], rcz.at[src, h])
        to_z(src, h, (src < z) & (z < Z - 1), (src > z) & (z > 0))
        to_x(src, h)
        to_core(src, h, t, 0)

    def from_x(d, h):
        src = src_of(d)
        got(car.at[src, xp, half(h)], scx.at[src, h], rcx.at[src, h])
        to_core(src, h, xp, 1)

    swap(1)
    for h in range(H):
        from_x(0, h)
    for d in range(1, Z):
        for h in range(H):
            arrive(d, h)
            if d > 1:
                from_x(d - 1, h)
        swap_one(2, d)
    for h in range(H):
        from_x(Z - 1, h)
    swapped(1)

    def up(d, h):
        src = src_of(d)
        hs = half(h)
        got(car.at[src, cp, hs], scc.at[src, 0, h], rcc.at[src, 0, h])
        got(car.at[src, cxp, hs], scc.at[src, 1, h], rcc.at[src, 1, h])
        total = jnp.zeros((hr, 1), f32)
        for q in range(T):
            c = car[src, q, hs].astype(f32)
            total += jnp.sum(c * c, axis=-1, keepdims=True)
        scale = lax.rsqrt(total / D + norm_eps)
        for q in range(T):
            part = slice(q * own, (q + 1) * own)
            xn[:, part] = (car[src, q, hs].astype(f32) * scale * lg[:, part]).astype(bf)
        pre = jnp.dot(xn[...], upg[...], preferred_element_type=f32)
        pre = jnp.maximum(pre * us[:, pl.ds(mul(z, fsub), fsub)], 0.0)
        hid[src, hs] = (pre * pre).astype(bf)

    def down(d, h):
        src = src_of(d)
        hs = half(h)
        hidden = hid[src, hs]
        for q in range(T):
            part = slice(q * own, (q + 1) * own)
            p = jnp.dot(hidden, dng[q], preferred_element_type=f32) * ds[:, part]
            pb[src, q, hs] = p.astype(bf)
        for k, q in ((1, cxp), (0, cp)):
            send(pb.at[src, q, hs], ra.at[src, k, hs], sa.at[src, k, h], ra_s.at[src, k, h], (r, z, cp))

    def over_x(d, h):
        src = src_of(d)
        hs = half(h)
        got(ra.at[src, 1, hs], sa.at[src, 1, h], ra_s.at[src, 1, h])
        sx[src, hs] = (pb[src, xp, hs].astype(f32) + ra[src, 1, hs].astype(f32)).astype(bf)
        send(sx.at[src, hs], rb.at[src, hs], sb.at[src, h], rb_s.at[src, h], (r, z, xp))

    def over_z(d, h):
        src = src_of(d)
        hs = half(h)
        got(ra.at[src, 0, hs], sa.at[src, 0, h], ra_s.at[src, 0, h])
        got(rb.at[src, hs], sb.at[src, h], rb_s.at[src, h])
        both = pb[src, t, hs].astype(f32) + ra[src, 0, hs].astype(f32) + rb[src, hs].astype(f32)
        if d == 0:
            return both
        sz[src, hs] = both.astype(bf)
        send(sz.at[src, hs], rc.at[z, hs], st.at[src, h], rt.at[z, h], (r, src, t))

    for d in range(Z):
        for h in range(H):
            up(d, h)
    swapped(2)
    units = [(d, h) for d in range(Z - 1, -1, -1) for h in range(H)]
    stages = (down, over_x, over_z)
    for i in range(len(units) + len(stages) - 1):
        for lag, stage in enumerate(stages):
            if 0 <= i - lag < len(units):
                d, h = units[i - lag]
                if d > 0 or stage is not over_z:
                    stage(d, h)

    writes = []

    def write(q, k, h):
        c = pltpu.make_async_copy(
            og.at[q, half(h)], out_h.at[half(h), pl.ds(mul(q, own), own)], wr.at[k, h]
        )
        c.start()
        writes.append(c)

    def pass_on(q, k, dev, h):
        b = og.at[q, half(h)]
        send(b, b, so.at[k, h], ro.at[k, h], dev)

    for h in range(H):
        hs = half(h)
        acc = over_z(0, h) + car[z, t, hs].astype(f32)
        for d in range(1, Z):
            src = src_of(d)
            got(rc.at[src, hs], st.at[src, h], rt.at[src, h])
            acc += rc[src, hs].astype(f32)
        og[t, hs] = acc.astype(bf)
        pass_on(t, 0, (r, z, xp), h)
        pass_on(t, 1, (r, z, cp), h)
        write(t, 0, h)
    for h in range(H):
        got(og.at[xp, half(h)], so.at[0, h], ro.at[0, h])
        pass_on(xp, 2, (r, z, cp), h)
        write(xp, 1, h)
    for h in range(H):
        got(og.at[cp, half(h)], so.at[1, h], ro.at[1, h])
        write(cp, 2, h)
        got(og.at[cxp, half(h)], so.at[2, h], ro.at[2, h])
        write(cxp, 3, h)
    drain()
    for c in writes:
        c.wait()


def fused(mesh_shape, tokens, mix_gain, group_weight, group_scale, mlp_gain, up_weight, up_scale, down_weight, down_scale):
    Z, T = mesh_shape["fs"], mesh_shape["tp"]
    rows, D = tokens.shape
    own = group_weight.shape[1]
    hg, hu = group_weight.shape[0] // 2, up_weight.shape[0] // 2
    fsub = up_weight.shape[1] // Z
    hd = fsub // 2
    dsub = down_weight.shape[1]
    bf, f32 = jnp.bfloat16, jnp.float32
    dma = pltpu.SemaphoreType.DMA
    vm = pl.BlockSpec(memory_space=pltpu.VMEM)
    hbm = pl.BlockSpec(memory_space=pl.ANY)
    sizes = (Z, T, rows, D, own, hg, hu, hd, fsub, dsub)
    V = pltpu.VMEM
    block = (Z, rows, own)
    H = rows // LENGTH
    return pl.pallas_call(
        functools.partial(ring_kernel, sizes),
        out_shape=jax.ShapeDtypeStruct((rows, D), bf),
        in_specs=[hbm, vm, hbm, vm, vm, hbm, vm, hbm, vm],
        out_specs=hbm,
        scratch_shapes=[
            V((rows, D), bf), V((2 * hg, own), f32),
            V((Z, hu, fsub), f32), V((hu, fsub), f32), V((Z, hd, dsub), f32), V((hd, dsub), f32),
            V((Z * 2 * hg, own), bf), V((Z, hu, fsub), bf), V((Z * 2 * hu, fsub), bf),
            V((Z, hd, dsub), bf), V((Z, 2 * hd, dsub), bf),
            V((Z, T, rows, own), bf), V((LENGTH, D), bf), V((Z, rows, fsub), bf), V((Z, T, rows, own), bf),
            V((Z, 2, rows, own), bf), V(block, bf), V(block, bf), V(block, bf), V(block, bf),
            V((T, rows, own), bf),
            dma((4 + 2 * Z,)), dma((3, Z)), dma((3, Z)), dma((3, Z)), dma((3, Z)),
            dma((2, Z, H)), dma((Z, H)), dma((Z, H)), dma((Z, H)), dma((Z, 2, H)), dma((Z, 2, H)),
            dma((Z, 2, H)), dma((Z, 2, H)), dma((Z, H)), dma((Z, H)), dma((Z, H)), dma((Z, H)),
            dma((3, H)), dma((3, H)), dma((4, H)),
        ],
        compiler_params=pltpu.CompilerParams(
            collective_id=0, has_side_effects=True, vmem_limit_bytes=60 * 1024 * 1024
        ),
    )(
        tokens, mix_gain[None], group_weight, group_scale, mlp_gain[None],
        up_weight, up_scale, down_weight, down_scale,
    )


def fits(mesh):
    shape = mesh.shape
    return shape["rep"] == 2 and shape["tp"] == GROUPS and shape["fs"] == shape["tp"]


def solution(mesh):
    in_specs = (
        P(("rep", "fs"), None),
        P(),
        P("fs", "tp"),
        P(None, "tp"),
        P(),
        P("fs", "tp"),
        P(None, "tp"),
        P("tp", "fs"),
        P(),
    )
    out_specs = P(("rep", "fs"), None)
    chosen = functools.partial(fused, mesh.shape) if fits(mesh) else body
    return jax.shard_map(chosen, mesh=mesh, in_specs=in_specs, out_specs=out_specs, check_vma=False)
```

profile of v0, /device:TPU:1, one launch (start us, length us, event | category | flops | bytes accessed | tf_op | source)
XLA Modules:
  0.0 120.5 jit_solution(1050311871532785350)
XLA Ops:
  0.0 118.2 %shard_map.91 = bf16[256,2048]{1,0:T(8,128)(2,1)} custom-call(bf16[256,2048]{1,0:T(8,128)(2,1)} %tok_h.1, f32[1,2048]{1,0:T(1,128)} %bitcast.2, f32[128,512]{1,0:T(8,128)} %gw_h.1, f32[1,512]{1,0:T(1,128)} %gs.1, f32[1,2048]{1,0:T(1,128)} %bitcast.3, f32[512,2048]{1,0:T(8,128)} %up_h.1, f32[1,2048]{1,0:T(1,128)} %us.1, f32[2048,512]{1,0:T(8,128)} %dn_h.1, ...), custom_call_target="tpu_custom_call" | custom-call | tf_op jit(solution)/shard_map/pallas_call | solution.py:408
  118.2 2.3 %copy.11 = bf16[256,2048]{1,0:T(8,128)(2,1)} copy(bf16[256,2048]{1,0:T(8,128)(2,1)} %shard_map.91) | data formatting | bytes 2097152
where the time goes:
time: 121 us; the launch traced here: 120 us
  Pallas kernels  118 us (98%)
  local copies, waits for them, and re-layouts  2.3 us (2%)
    pallas_call x1, Pallas kernels, fused(): pl.pallas_call(functools.partial(ring_kernel, sizes), out_shape=jax.Shape...  118 us

commit v1 on v0

v1 whole, which is shorter than its diff:
```python
import functools

import jax
import jax.numpy as jnp
from jax import lax
from jax.experimental import pallas as pl
from jax.experimental.pallas import tpu as pltpu
from jax.sharding import PartitionSpec as P

GROUPS = 4
LENGTH = 128


norm_eps = 1e-06


def norm_rows(values, gain):
    promoted = values.astype(jnp.float32)
    inverse = lax.rsqrt(jnp.mean(promoted * promoted, axis=-1, keepdims=True) + norm_eps)
    return (promoted * inverse * gain).astype(jnp.bfloat16)


def band_means(inputs, window, seq_length):
    row_count, columns = inputs.shape
    by_sequence = inputs.reshape(row_count // seq_length, seq_length, columns)
    position = jnp.arange(seq_length, dtype=jnp.int32)
    offset = position[:, None] - position[None, :]
    band_mask = ((offset >= 0) & (offset < window)).astype(jnp.bfloat16)
    divisor = jnp.minimum(position + 1, window).astype(jnp.float32)
    summed = jnp.einsum("ts,nsc->ntc", band_mask, by_sequence, preferred_element_type=jnp.float32)
    return (summed / divisor[None, :, None] - by_sequence.astype(jnp.float32)).reshape(
        row_count, columns
    )


def body(
    tokens,
    mix_gain,
    group_weight,
    group_scale,
    mlp_gain,
    up_weight,
    up_scale,
    down_weight,
    down_scale,
):
    model_width = tokens.shape[1]
    group_width = model_width // GROUPS
    own_cols = group_weight.shape[1]
    column_start = lax.axis_index("tp") * own_cols
    group_index = column_start // group_width
    normed = norm_rows(tokens, mix_gain)
    inputs = lax.dynamic_slice_in_dim(normed, group_index * group_width, group_width, 1)
    window = jnp.left_shift(jnp.int32(2), group_index)
    pooled = band_means(inputs, window, LENGTH).astype(jnp.bfloat16)
    mixed_cols = (
        jnp.dot(
            pooled,
            lax.all_gather(group_weight.astype(jnp.bfloat16), "fs", axis=0, tiled=True),
            preferred_element_type=jnp.float32,
        )
        * group_scale
    )
    own_tokens = lax.dynamic_slice_in_dim(tokens, column_start, own_cols, 1)
    carried_cols = (own_tokens.astype(jnp.float32) + mixed_cols).astype(jnp.bfloat16)
    carried = lax.all_gather(carried_cols, "tp", axis=1, tiled=True)
    normed_mlp = norm_rows(carried, mlp_gain)
    pre_act = (
        jnp.dot(
            normed_mlp,
            lax.all_gather(up_weight.astype(jnp.bfloat16), "fs", axis=0, tiled=True),
            preferred_element_type=jnp.float32,
        )
        * up_scale
    )
    hidden = jnp.square(jax.nn.relu(pre_act)).astype(jnp.bfloat16)
    partial_value = (
        jnp.dot(
            hidden,
            lax.all_gather(down_weight.astype(jnp.bfloat16), "fs", axis=1, tiled=True),
            preferred_element_type=jnp.float32,
        )
        * down_scale
    )
    summed = lax.psum(partial_value.astype(jnp.bfloat16), "tp").astype(jnp.float32)
    return (carried.astype(jnp.float32) + summed).astype(jnp.bfloat16)


MESH = pl.DeviceIdType.MESH
CHUNKS = 4
PARTS = 2


def ring_kernel(
    sizes,
    tok_h, mg, gw_h, gs, lg, up_h, us, dn_h, ds,
    out_h,
    tok, gwf, upf, upo, dnf, dno,
    gwg, ups, upg, dns, dng,
    car, xn, hid, pb, ra, sx, rb, sz, ri, rc, og,
    ld, sw, rw, sy, ry, swu, rwu, syu, ryu, swd, rwd, syd, ryd, scz, rcz, scx, rcx, scc, rcc,
    sa, ra_s, sb, rb_s, st, rt, sm, rm, so, ro, wr,
):
    Z, T, C, rows, D, own, hg, hu, hd, fsub, dsub = sizes
    cw = dsub // C
    r, z, t = lax.axis_index("rep"), lax.axis_index("fs"), lax.axis_index("tp")
    cp = t + 1 - 2 * lax.rem(t, 2)
    xp = lax.rem(t + 2, T)
    cxp = lax.rem(cp + 2, T)
    peer_r = 1 - r
    bf, f32 = jnp.bfloat16, jnp.float32
    mate = z + 1 - 2 * lax.rem(z, 2)
    zk = (z, mate, lax.rem(z + 2, Z), Z - 1 - z)
    inner = (z > 0) & (z < Z - 1)
    outer = (z == 0) | (z == Z - 1)

    def mul(i, n):
        return pl.multiple_of(i * n, n)

    loads = {}

    def load(key, src, dst, k):
        c = pltpu.make_async_copy(src, dst, ld.at[k])
        c.start()
        loads[key] = c

    def load_up(k):
        load(("up", k), up_h.at[pl.ds(mul(r, hu), hu), pl.ds(mul(zk[k], fsub), fsub)], upf.at[k], 2 + k)

    def load_dn(k):
        load(("dn", k), dn_h.at[pl.ds(pl.multiple_of(zk[k] * 2 * hd + r * hd, hd), hd), :], dnf.at[k], 2 + Z + k)

    load("gw", gw_h, gwf, 0)
    load_up(2)
    load("tok", tok_h, tok, 1)
    load_up(3)
    load_up(1)
    load_up(0)
    load("upo", up_h.at[pl.ds(mul(peer_r, hu), hu), pl.ds(mul(z, fsub), fsub)], upo, 2 + 2 * Z)
    for k in (2, 3, 1, 0):
        load_dn(k)
    load("dno", dn_h.at[pl.ds(pl.multiple_of(z * 2 * hd + peer_r * hd, hd), hd), :], dno, 3 + 2 * Z)

    barrier = pltpu.get_barrier_semaphore()
    peers = [(r, zk[k], t) for k in range(1, Z)] + [(peer_r, z, t), (r, z, xp), (r, z, cp)]
    for p in peers:
        pl.semaphore_signal(barrier, inc=1, device_id=p, device_id_type=MESH)
    loads["gw"].wait()
    gwg[pl.ds(mul(z, 2 * hg), 2 * hg), :] = gwf[...].astype(bf)
    loads[("up", 2)].wait()
    ups[2] = upf[2].astype(bf)
    with jax.named_scope("barrier"):
        pl.semaphore_wait(barrier, len(peers))

    sends = []

    def remote(src, dst, ss, rs, dev):
        return pltpu.make_async_remote_copy(
            src_ref=src, dst_ref=dst, send_sem=ss, recv_sem=rs, device_id=dev, device_id_type=MESH
        )

    role = [None]

    def guarded(fn, when=None):
        for p in (role[0],):
            if p is not None:
                when = p if when is None else when & p
        if when is None:
            fn()
        else:
            pl.when(when)(fn)
        return when

    def send(src, dst, ss, rs, dev, when=None):
        when = guarded(lambda: remote(src, dst, ss, rs, dev).start(), when)
        sends.append((when, (src, dst, ss, rs, dev)))

    def drain():
        for when, args in sends:
            if when is None:
                remote(*args).wait_send()
            else:
                pl.when(when)(lambda args=args: remote(*args).wait_send())

    def got(dst, ss, rs):
        guarded(lambda: remote(dst, dst, ss, rs, (peer_r, z, t)).wait_recv())

    def only(who, *steps):
        role[0] = who
        for name, fn, *args in steps:
            run(name, fn, *args)
        role[0] = None

    def run(name, fn, *args):
        with jax.named_scope(name + "".join(map(str, [a for a in args if isinstance(a, int)]))):
            fn(*args)

    def gw_at(src, rep):
        return gwg.at[pl.ds(pl.multiple_of(src * 2 * hg + rep * hg, hg), hg), :]

    pu = hu // PARTS

    def up_at(src, rep, i):
        return upg.at[pl.ds(pl.multiple_of(src * 2 * hu + rep * hu + i * pu, pu), pu), :]

    def dn_at(c, src, rep):
        return dng.at[c, pl.ds(mul(rep, hd), hd), pl.ds(mul(src, cw), cw)]

    def up_send(k, when=None):
        for i in range(PARTS):
            piece = ups.at[k, pl.ds(i * pu, pu)]
            send(piece, up_at(z, r, i), swu.at[k, i], rwu.at[z, i], (r, zk[k], t), when)

    def dn_send(c, k, when=None):
        send(dns.at[k, c], dn_at(c, z, r), swd.at[c, k], rwd.at[c, z], (r, zk[k], t), when)

    for k in (3, 2, 1):
        send(gw_at(z, r), gw_at(z, r), sw.at[k], rw.at[z], (r, zk[k], t))
    loads[("up", 3)].wait()
    ups[3] = upf[3].astype(bf)
    loads[("up", 1)].wait()
    ups[1] = upf[1].astype(bf)
    up_send(2, inner)
    up_send(3, inner)
    up_send(1)

    loads["tok"].wait()
    full = tok[...].astype(f32)
    inv = lax.rsqrt(jnp.mean(full * full, axis=-1, keepdims=True) + norm_eps)
    cols = pl.ds(mul(t, own), own)
    mine = tok[:, cols].astype(f32)
    normed = (mine * inv * mg[:, cols]).astype(bf)
    window = jnp.left_shift(jnp.int32(2), t)
    ti = lax.broadcasted_iota(jnp.int32, (LENGTH, LENGTH), 0)
    si = lax.broadcasted_iota(jnp.int32, (LENGTH, LENGTH), 1)
    band = jnp.where((ti - si >= 0) & (ti - si < window), 1.0, 0.0).astype(bf)
    pos = lax.broadcasted_iota(jnp.int32, (LENGTH, own), 0)
    divisor = jnp.minimum(pos + 1, window).astype(f32)
    for s in range(rows // LENGTH):
        part = normed[s * LENGTH:(s + 1) * LENGTH]
        summed = jnp.dot(band, part, preferred_element_type=f32)
        xn[s * LENGTH:(s + 1) * LENGTH, :own] = (summed / divisor - part.astype(f32)).astype(bf)

    def gw_swap(src):
        got(gw_at(src, r), sw.at[0], rw.at[src])
        send(gw_at(src, r), gw_at(src, r), sy.at[src], ry.at[src], (peer_r, z, t))

    def up_swap(src):
        for i in range(PARTS):
            b = up_at(src, r, i)
            got(b, swu.at[0, i], rwu.at[src, i])
            send(b, b, syu.at[src, i], ryu.at[src, i], (peer_r, z, t))

    def up_swapped(src):
        for i in range(PARTS):
            got(up_at(src, peer_r, i), syu.at[src, i], ryu.at[src, i])

    for k in (3, 2):
        loads[("dn", k)].wait()
        dns[k, 0] = dnf[k, :, :cw].astype(bf)
    with jax.named_scope("gwswap"):
        gw_swap(zk[1])
        for k in (2, 3):
            gw_swap(zk[k])
        up_send(3, outer)
        up_send(2, outer)
        dn_send(0, 3, outer)
        dn_send(0, 2, outer)
    with jax.named_scope("gwswapped"):
        for k in (1, 2, 3):
            got(gw_at(zk[k], peer_r), sy.at[zk[k]], ry.at[zk[k]])
    with jax.named_scope("mix"):
        mixed = jnp.dot(xn[:, :own], gwg[...], preferred_element_type=f32) * gs[...]
        car[z, t] = (tok[:, cols].astype(f32) + mixed).astype(bf)
    H = rows // LENGTH
    hr = LENGTH
    low = 1 - lax.div(z, Z // 2)
    near, far = 1 + low, 3 * low
    blocks = (z, mate, near, far)
    def half(h):
        return pl.ds(h * hr, hr)

    def to_x(src, h):
        b = car.at[src, t, half(h)]
        send(b, b, scx.at[src, h], rcx.at[src, h], (r, z, xp))

    def to_core(src, h, q, k):
        b = car.at[src, q, half(h)]
        send(b, b, scc.at[src, k, h], rcc.at[src, k, h], (r, z, cp))

    def to_z(src, h, when_up, when_down):
        b = car.at[src, t, half(h)]
        send(b, b, scz.at[0, src, h], rcz.at[src, h], (r, lax.rem(z + 1, Z), t), when_up)
        send(b, b, scz.at[1, src, h], rcz.at[src, h], (r, lax.rem(z + Z - 1, Z), t), when_down)

    for h in range(H):
        to_z(z, h, z < Z - 1, z > 0)
        to_x(z, h)
        to_core(z, h, t, 0)
    with jax.named_scope("casts"):
        for k in (2, 3, 1):
            if k == 1:
                loads[("dn", 1)].wait()
            for c in range(int(k != 1), C):
                dns[k, c] = dnf[k, :, c * cw:(c + 1) * cw].astype(bf)
        loads[("up", 0)].wait()
        upg[pl.ds(pl.multiple_of(z * 2 * hu + r * hu, hu), hu), :] = upf[0].astype(bf)
        loads["upo"].wait()
        upg[pl.ds(pl.multiple_of(z * 2 * hu + peer_r * hu, hu), hu), :] = upo[...].astype(bf)
        loads[("dn", 0)].wait()
        loads["dno"].wait()
        for c in range(C):
            here = pl.ds(mul(z, cw), cw)
            dng[c, pl.ds(mul(r, hd), hd), here] = dnf[0, :, c * cw:(c + 1) * cw].astype(bf)
            dng[c, pl.ds(mul(peer_r, hd), hd), here] = dno[:, c * cw:(c + 1) * cw].astype(bf)

    def arrive(d, h):
        src = blocks[d]
        got(car.at[src, t, half(h)], scz.at[0, src, h], rcz.at[src, h])
        to_z(src, h, (src < z) & (z < Z - 1), (src > z) & (z > 0))
        to_x(src, h)
        to_core(src, h, t, 0)

    def from_x(d, h):
        src = blocks[d]
        got(car.at[src, xp, half(h)], scx.at[src, h], rcx.at[src, h])
        to_core(src, h, xp, 1)

    def dn_group(*pieces):
        for c, k in pieces:
            dn_send(c, k)

    def dn_outer(c):
        dn_group((c, 3), (c, 2), (c, 1))

    def dn_early():
        dn_group((0, 3), (1, 3))

    def dn_rest():
        dn_group((2, 3), (1, 1))

    def far_core():
        for h in range(H):
            got(car.at[far, cp, half(h)], scc.at[far, 0, h], rcc.at[far, 0, h])

    def dn_forward(c, k):
        src = zk[k]
        got(dn_at(c, src, r), swd.at[c, k], rwd.at[c, src])
        send(dn_at(c, src, r), dn_at(c, src, r), syd.at[c, k], ryd.at[c, src], (peer_r, z, t))

    def up(d):
        src = blocks[d]
        for h in range(H):
            hs = half(h)
            if d < 3:
                got(car.at[src, cp, hs], scc.at[src, 0, h], rcc.at[src, 0, h])
            got(car.at[src, cxp, hs], scc.at[src, 1, h], rcc.at[src, 1, h])
        total = jnp.zeros((rows, 1), f32)
        for q in range(T):
            c = car[src, q].astype(f32)
            total += jnp.sum(c * c, axis=-1, keepdims=True)
        scale = lax.rsqrt(total / D + norm_eps)
        for q in range(T):
            part = slice(q * own, (q + 1) * own)
            xn[:, part] = (car[src, q].astype(f32) * scale * lg[:, part]).astype(bf)
        pre = jnp.dot(xn[...], upg[...], preferred_element_type=f32)
        pre = jnp.maximum(pre * us[:, pl.ds(mul(z, fsub), fsub)], 0.0)
        hid[src] = (pre * pre).astype(bf)

    def dn_ready(c):
        for k in range(1, Z):
            src = zk[k]
            got(dn_at(c, src, peer_r), syd.at[c, k], ryd.at[c, src])

    def down(c, k):
        src = zk[k]
        p = jnp.dot(hid[src], dng[c], preferred_element_type=f32)
        for q in range(T):
            part = p[:, q * cw:(q + 1) * cw] * ds[:, q * own + c * cw:q * own + (c + 1) * cw]
            pb[c, src, q] = part.astype(bf)
        for j, q in ((1, cxp), (0, cp)):
            send(pb.at[c, src, q], ra.at[c, src, j], sa.at[c, src, j], ra_s.at[c, src, j], (r, z, cp))

    def over_x(c, k):
        src = zk[k]
        got(ra.at[c, src, 1], sa.at[c, src, 1], ra_s.at[c, src, 1])
        sx[c, src] = (pb[c, src, xp].astype(f32) + ra[c, src, 1].astype(f32)).astype(bf)
        send(sx.at[c, src], rb.at[c, src], sb.at[c, src], rb_s.at[c, src], (r, z, xp))

    def both(c, src):
        return pb[c, src, t].astype(f32) + ra[c, src, 0].astype(f32) + rb[c, src].astype(f32)

    def joined(c, k):
        src = zk[k]
        got(ra.at[c, src, 0], sa.at[c, src, 0], ra_s.at[c, src, 0])
        got(rb.at[c, src], sb.at[c, src], rb_s.at[c, src])

    def to_inner(c, k):
        src = zk[k]
        joined(c, k)

        @pl.when(outer)
        def _():
            sz[c, src] = both(c, src).astype(bf)

        send(sz.at[c, src], ri.at[c, src], sm.at[c, src], rm.at[c, src], (r, mate, t), outer)

    def across(c, k):
        src = zk[k]

        @pl.when(inner)
        def _():
            got(ri.at[c, src], sm.at[c, src], rm.at[c, src])
            sz[c, src] = (both(c, src) + ri[c, src].astype(f32)).astype(bf)

        send(sz.at[c, src], rc.at[c, 1], st.at[c, src], rt.at[c, 1], (r, src, t), inner)

    def to_mate(c):
        joined(c, 1)
        sz[c, mate] = both(c, mate).astype(bf)
        send(sz.at[c, mate], rc.at[c, 0], st.at[c, mate], rt.at[c, 0], (r, mate, t))

    writes = []

    def write(c, q, j):
        cc = pltpu.make_async_copy(
            og.at[c, q], out_h.at[:, pl.ds(pl.multiple_of(q * own + c * cw, cw), cw)], wr.at[c, j]
        )
        cc.start()
        writes.append(cc)

    def pass_on(c, q, j, dev):
        b = og.at[c, q]
        send(b, b, so.at[c, j], ro.at[c, j], dev)

    def finish(c):
        joined(c, 0)
        acc = both(c, z) + car[z, t, :, :].astype(f32)[:, c * cw:(c + 1) * cw]
        for j in range(2):
            got(rc.at[c, j], st.at[c, z], rt.at[c, j])
            acc += rc[c, j].astype(f32)
        og[c, t] = acc.astype(bf)
        pass_on(c, t, 0, (r, z, xp))
        pass_on(c, t, 1, (r, z, cp))
        write(c, t, 0)

    def spread(c):
        got(og.at[c, xp], so.at[c, 0], ro.at[c, 0])
        pass_on(c, xp, 2, (r, z, cp))
        write(c, xp, 1)

    def collect(c):
        got(og.at[c, cp], so.at[c, 1], ro.at[c, 1])
        write(c, cp, 2)
        got(og.at[c, cxp], so.at[c, 2], ro.at[c, 2])
        write(c, cxp, 3)

    def up_ready():
        for k in (1, 2, 3):
            up_swapped(zk[k])

    run("us1", up_swap, zk[1])
    for h in range(H):
        run("fx", from_x, 0, h)
    only(outer, ("ous3", up_swap, zk[3]))
    only(inner, ("ius2", up_swap, zk[2]))
    for h in range(H):
        run("arr", arrive, 1, h)
    only(inner, ("dn", dn_early), ("ius3", up_swap, zk[3]), ("ifwd", dn_forward, 0, 2))
    for h in range(H):
        run("fx", from_x, 1, h)
    only(outer, ("ous2", up_swap, zk[2]))
    for h in range(H):
        run("arr", arrive, 2, h)
    only(outer, ("dn", dn_group, (0, 1)), ("ofwd", dn_forward, 0, 3))
    run("usd", up_ready)
    for h in range(H):
        run("fx", from_x, 2, h)
    run("up", up, 0)
    run("up", up, 1)
    for h in range(H):
        run("arr", arrive, 3, h)
    only(inner, ("dn", dn_group, (0, 1)))
    run("up", up, 2)
    for h in range(H):
        run("fx", from_x, 3, h)
    only(inner, ("dn", dn_rest))
    run("far", far_core)
    only(outer, ("dn", dn_group, (1, 3), (1, 2), (1, 1)))
    run("fwd", dn_forward, 0, 1)
    only(inner, ("ifwd", dn_forward, 0, 3), ("dn", dn_group, (0, 2), (1, 2)))
    only(outer, ("ofwd", dn_forward, 0, 2))
    run("up", up, 3)

    def forward(c):
        for k in (1, 2, 3):
            run("fwd", dn_forward, c, k)

    only(outer, ("dn", dn_outer, 2))
    only(inner, ("dn", dn_group, (2, 2), (2, 1), (3, 3)))
    for c in range(C):
        run("ready", dn_ready, c)
        for k in (3, 2, 1, 0):
            run("down", down, c, k)
        if c > 0:
            for k in (3, 2):
                run("inner", to_inner, c - 1, k)
        for k in (3, 2, 1, 0):
            run("x", over_x, c, k)
        if c == 0:
            forward(1)
            only(outer, ("dn", dn_outer, 3))
            only(inner, ("dn", dn_group, (3, 2), (3, 1)))
        if c + 2 < C:
            forward(c + 2)
        if c > 0:
            run("mate", to_mate, c - 1)
            for k in (3, 2):
                run("across", across, c - 1, k)
        if c > 1:
            run("fin", finish, c - 2)
    for k in (3, 2):
        run("inner", to_inner, C - 1, k)
    for c in range(C - 2):
        run("spread", spread, c)
    for k in (3, 2):
        run("across", across, C - 1, k)
    run("mate", to_mate, C - 1)
    run("fin", finish, C - 2)
    for c in range(C - 2):
        run("coll", collect, c)
    run("fin", finish, C - 1)
    for c in (C - 2, C - 1):
        run("spread", spread, c)
    for c in (C - 2, C - 1):
        run("coll", collect, c)
    with jax.named_scope("drain"):
        drain()
        for c in writes:
            c.wait()


def fused(mesh_shape, tokens, mix_gain, group_weight, group_scale, mlp_gain, up_weight, up_scale, down_weight, down_scale):
    Z, T = mesh_shape["fs"], mesh_shape["tp"]
    C = CHUNKS
    rows, D = tokens.shape
    own = group_weight.shape[1]
    hg, hu = group_weight.shape[0] // 2, up_weight.shape[0] // 2
    fsub = up_weight.shape[1] // Z
    hd = fsub // 2
    dsub = down_weight.shape[1]
    cw = dsub // C
    bf, f32 = jnp.bfloat16, jnp.float32
    dma = pltpu.SemaphoreType.DMA
    vm = pl.BlockSpec(memory_space=pltpu.VMEM)
    hbm = pl.BlockSpec(memory_space=pl.ANY)
    sizes = (Z, T, C, rows, D, own, hg, hu, hd, fsub, dsub)
    V = pltpu.VMEM
    H = rows // LENGTH
    piece = (C, Z, rows, cw)
    return pl.pallas_call(
        functools.partial(ring_kernel, sizes),
        out_shape=jax.ShapeDtypeStruct((rows, D), bf),
        in_specs=[hbm, vm, hbm, vm, vm, hbm, vm, hbm, vm],
        out_specs=hbm,
        scratch_shapes=[
            V((rows, D), bf), V((2 * hg, own), f32),
            V((Z, hu, fsub), f32), V((hu, fsub), f32), V((Z, hd, dsub), f32), V((hd, dsub), f32),
            V((Z * 2 * hg, own), bf), V((Z, hu, fsub), bf), V((Z * 2 * hu, fsub), bf),
            V((Z, C, hd, cw), bf), V((C, 2 * hd, Z * cw), bf),
            V((Z, T, rows, own), bf), V((rows, D), bf), V((Z, rows, fsub), bf), V((C, Z, T, rows, cw), bf),
            V((C, Z, 2, rows, cw), bf), V(piece, bf), V(piece, bf), V(piece, bf), V(piece, bf),
            V((C, 2, rows, cw), bf), V((C, T, rows, cw), bf),
            dma((4 + 2 * Z,)), dma((Z,)), dma((Z,)), dma((Z,)), dma((Z,)),
            dma((Z, PARTS)), dma((Z, PARTS)), dma((Z, PARTS)), dma((Z, PARTS)),
            dma((C, Z)), dma((C, Z)), dma((C, Z)), dma((C, Z)),
            dma((2, Z, H)), dma((Z, H)), dma((Z, H)), dma((Z, H)), dma((Z, 2, H)), dma((Z, 2, H)),
            dma((C, Z, 2)), dma((C, Z, 2)), dma((C, Z)), dma((C, Z)), dma((C, Z)), dma((C, 2)),
            dma((C, Z)), dma((C, Z)), dma((C, 3)), dma((C, 3)), dma((C, 4)),
        ],
        compiler_params=pltpu.CompilerParams(
            collective_id=0, has_side_effects=True, vmem_limit_bytes=60 * 1024 * 1024
        ),
    )(
        tokens, mix_gain[None], group_weight, group_scale, mlp_gain[None],
        up_weight, up_scale, down_weight, down_scale,
    )


def fits(mesh):
    shape = mesh.shape
    return shape["rep"] == 2 and shape["tp"] == GROUPS and shape["fs"] == shape["tp"]


def solution(mesh):
    in_specs = (
        P(("rep", "fs"), None),
        P(),
        P("fs", "tp"),
        P(None, "tp"),
        P(),
        P("fs", "tp"),
        P(None, "tp"),
        P("tp", "fs"),
        P(),
    )
    out_specs = P(("rep", "fs"), None)
    chosen = functools.partial(fused, mesh.shape) if fits(mesh) else body
    return jax.shard_map(chosen, mesh=mesh, in_specs=in_specs, out_specs=out_specs, check_vma=False)
```

time: 121 us -> 116 us (0.959)
  Pallas kernels: 118 us -> 113 us
    pallas_call x1, Pallas kernels: 118 us -> 113 us  [fused(): pl.pallas_call(functools.partial(ring_kernel, sizes), out_shape=jax.Shape...]
where the time goes in v1:
time: 116 us; the launch traced here: 115 us
  Pallas kernels  113 us (97%)
  local copies, waits for them, and re-layouts  2.3 us (2%)
    pallas_call x1, Pallas kernels, fused(): pl.pallas_call(functools.partial(ring_kernel, sizes), out_shape=jax.Shape...  113 us

profile of v1, /device:TPU:1, one launch (start us, length us, event | category | flops | bytes accessed | tf_op | source)
XLA Modules:
  0.0 115.4 jit_solution(10027067419553665748)
XLA Ops:
  0.0 113.1 %shard_map.91 = bf16[256,2048]{1,0:T(8,128)(2,1)} custom-call(bf16[256,2048]{1,0:T(8,128)(2,1)} %tok_h.1, f32[1,2048]{1,0:T(1,128)} %bitcast.2, f32[128,512]{1,0:T(8,128)} %gw_h.1, f32[1,512]{1,0:T(1,128)} %gs.1, f32[1,2048]{1,0:T(1,128)} %bitcast.3, f32[512,2048]{1,0:T(8,128)} %up_h.1, f32[1,2048]{1,0:T(1,128)} %us.1, f32[2048,512]{1,0:T(8,128)} %dn_h.1, ...), custom_call_target="tpu_custom_call" | custom-call | tf_op jit(solution)/shard_map/pallas_call | solution.py:561
  113.1 2.3 %copy.11 = bf16[256,2048]{1,0:T(8,128)(2,1)} copy(bf16[256,2048]{1,0:T(8,128)(2,1)} %shard_map.91) | data formatting | bytes 2097152

commit v2 on v1

v2 whole, which is shorter than its diff:
```python
import functools

import jax
import jax.numpy as jnp
from jax import lax
from jax.experimental import pallas as pl
from jax.experimental.pallas import tpu as pltpu
from jax.sharding import PartitionSpec as P

GROUPS = 4
LENGTH = 128


norm_eps = 1e-06


def norm_rows(values, gain):
    promoted = values.astype(jnp.float32)
    inverse = lax.rsqrt(jnp.mean(promoted * promoted, axis=-1, keepdims=True) + norm_eps)
    return (promoted * inverse * gain).astype(jnp.bfloat16)


def band_means(inputs, window, seq_length):
    row_count, columns = inputs.shape
    by_sequence = inputs.reshape(row_count // seq_length, seq_length, columns)
    position = jnp.arange(seq_length, dtype=jnp.int32)
    offset = position[:, None] - position[None, :]
    band_mask = ((offset >= 0) & (offset < window)).astype(jnp.bfloat16)
    divisor = jnp.minimum(position + 1, window).astype(jnp.float32)
    summed = jnp.einsum("ts,nsc->ntc", band_mask, by_sequence, preferred_element_type=jnp.float32)
    return (summed / divisor[None, :, None] - by_sequence.astype(jnp.float32)).reshape(
        row_count, columns
    )


def body(
    tokens,
    mix_gain,
    group_weight,
    group_scale,
    mlp_gain,
    up_weight,
    up_scale,
    down_weight,
    down_scale,
):
    model_width = tokens.shape[1]
    group_width = model_width // GROUPS
    own_cols = group_weight.shape[1]
    column_start = lax.axis_index("tp") * own_cols
    group_index = column_start // group_width
    normed = norm_rows(tokens, mix_gain)
    inputs = lax.dynamic_slice_in_dim(normed, group_index * group_width, group_width, 1)
    window = jnp.left_shift(jnp.int32(2), group_index)
    pooled = band_means(inputs, window, LENGTH).astype(jnp.bfloat16)
    mixed_cols = (
        jnp.dot(
            pooled,
            lax.all_gather(group_weight.astype(jnp.bfloat16), "fs", axis=0, tiled=True),
            preferred_element_type=jnp.float32,
        )
        * group_scale
    )
    own_tokens = lax.dynamic_slice_in_dim(tokens, column_start, own_cols, 1)
    carried_cols = (own_tokens.astype(jnp.float32) + mixed_cols).astype(jnp.bfloat16)
    carried = lax.all_gather(carried_cols, "tp", axis=1, tiled=True)
    normed_mlp = norm_rows(carried, mlp_gain)
    pre_act = (
        jnp.dot(
            normed_mlp,
            lax.all_gather(up_weight.astype(jnp.bfloat16), "fs", axis=0, tiled=True),
            preferred_element_type=jnp.float32,
        )
        * up_scale
    )
    hidden = jnp.square(jax.nn.relu(pre_act)).astype(jnp.bfloat16)
    partial_value = (
        jnp.dot(
            hidden,
            lax.all_gather(down_weight.astype(jnp.bfloat16), "fs", axis=1, tiled=True),
            preferred_element_type=jnp.float32,
        )
        * down_scale
    )
    summed = lax.psum(partial_value.astype(jnp.bfloat16), "tp").astype(jnp.float32)
    return (carried.astype(jnp.float32) + summed).astype(jnp.bfloat16)


MESH = pl.DeviceIdType.MESH
CHUNKS = 4
PARTS = 4


def ring_kernel(
    sizes,
    tok_h, mg, gw_h, gs, lg, up_h, us, dn_h, ds,
    out_h,
    tok, gwf, upf, upo, dnf, dno,
    gwg, ups, upg, dns, dng,
    car, xn, hid, pb, ra, sx, rb, sz, ri, rc, og,
    ld, sent, rw, ry, rwu, ryu, rwd, ryd, rcz, rcx, rcc, rx, rj, rb_s, rt, rm, ro, rq,
):
    Z, T, C, rows, D, own, hg, hu, hd, fsub, dsub = sizes
    cw = dsub // C
    r, z, t = lax.axis_index("rep"), lax.axis_index("fs"), lax.axis_index("tp")
    cp = t + 1 - 2 * lax.rem(t, 2)
    xp = lax.rem(t + 2, T)
    cxp = lax.rem(cp + 2, T)
    peer_r = 1 - r
    bf, f32 = jnp.bfloat16, jnp.float32
    mate = z + 1 - 2 * lax.rem(z, 2)
    zk = (z, mate, lax.rem(z + 2, Z), Z - 1 - z)
    inner = (z > 0) & (z < Z - 1)
    outer = (z == 0) | (z == Z - 1)

    def mul(i, n):
        return pl.multiple_of(i * n, n)

    loads = {}

    def load(key, src, dst, k):
        c = pltpu.make_async_copy(src, dst, ld.at[k])
        c.start()
        loads[key] = c

    def load_up(k):
        load(("up", k), up_h.at[pl.ds(mul(r, hu), hu), pl.ds(mul(zk[k], fsub), fsub)], upf.at[k], 2 + k)

    def load_dn(k):
        load(("dn", k), dn_h.at[pl.ds(pl.multiple_of(zk[k] * 2 * hd + r * hd, hd), hd), :], dnf.at[k], 2 + Z + k)

    load("gw", gw_h, gwf, 0)
    load_up(2)
    load("tok", tok_h, tok, 1)
    load_up(3)
    load_up(1)
    load_up(0)
    load("upo", up_h.at[pl.ds(mul(peer_r, hu), hu), pl.ds(mul(z, fsub), fsub)], upo, 2 + 2 * Z)
    for k in (2, 3, 1, 0):
        load_dn(k)
    load("dno", dn_h.at[pl.ds(pl.multiple_of(z * 2 * hd + peer_r * hd, hd), hd), :], dno, 3 + 2 * Z)

    barrier = pltpu.get_barrier_semaphore()
    peers = [(r, zk[k], t) for k in range(1, Z)] + [(peer_r, z, t), (r, z, xp), (r, z, cp)]
    for p in peers:
        pl.semaphore_signal(barrier, inc=1, device_id=p, device_id_type=MESH)
    loads["gw"].wait()
    gwg[pl.ds(mul(z, 2 * hg), 2 * hg), :] = gwf[...].astype(bf)
    loads[("up", 2)].wait()
    ups[2] = upf[2].astype(bf)
    with jax.named_scope("barrier"):
        pl.semaphore_wait(barrier, len(peers))

    def remote(src, dst, ss, rs, dev):
        return pltpu.make_async_remote_copy(
            src_ref=src, dst_ref=dst, send_sem=ss, recv_sem=rs, device_id=dev, device_id_type=MESH
        )

    role = [None]

    def guarded(fn, when=None):
        for p in (role[0],):
            if p is not None:
                when = p if when is None else when & p
        if when is None:
            fn()
        else:
            pl.when(when)(fn)
        return when

    groups = ("gw", "gwy", "up", "upy", "dn", "dny", "carz", "carx", "carc", "pb", "sx", "sz", "og")

    def send(src, dst, group, rs, dev, when=None):
        guarded(lambda: remote(src, dst, sent.at[groups.index(group)], rs, dev).start(), when)

    def drain():
        three = pl.ds(1, Z - 1)
        same = (
            gwg.at[pl.ds(0, (Z - 1) * hg)], gwg.at[pl.ds(0, (Z - 1) * hg)], ups.at[three], ups.at[three],
            dns.at[three], dns.at[three], car.at[0, three], car.at[0], car.at[pl.ds(0, 2)],
            ra, rb, og.at[:, three], og.at[:, three],
        )
        for i, ref in enumerate(same):
            remote(ref, ref, sent.at[i], rcc.at[0], (peer_r, z, t)).wait_send()
        pltpu.make_async_copy(out_h, out_h, sent.at[len(same)]).wait()

    def got(dst, rs):
        guarded(lambda: remote(dst, dst, sent.at[0], rs, (peer_r, z, t)).wait_recv())

    def only(who, *steps):
        role[0] = who
        for name, fn, *args in steps:
            run(name, fn, *args)
        role[0] = None

    def run(name, fn, *args):
        with jax.named_scope(name + "".join(map(str, [a for a in args if isinstance(a, int)]))):
            fn(*args)

    def gw_at(src, rep):
        return gwg.at[pl.ds(pl.multiple_of(src * 2 * hg + rep * hg, hg), hg), :]

    pu = hu // PARTS

    def up_at(src, rep, i):
        return upg.at[pl.ds(pl.multiple_of(src * 2 * hu + rep * hu + i * pu, pu), pu), :]

    def dn_at(c, src, rep):
        return dng.at[c, pl.ds(mul(rep, hd), hd), pl.ds(mul(src, cw), cw)]

    early, late = range(PARTS // 2), range(PARTS // 2, PARTS)
    whole = range(PARTS)

    def up_send(k, when=None, parts=whole):
        for i in parts:
            piece = ups.at[k, pl.ds(i * pu, pu)]
            send(piece, up_at(z, r, i), "up", rwu.at[k - 1, i], (r, zk[k], t), when)

    def dn_send(c, k):
        send(dns.at[k, c], dn_at(c, z, r), "dn", rwd.at[k - 1, c], (r, zk[k], t))

    for k in (3, 2, 1):
        send(gw_at(z, r), gw_at(z, r), "gw", rw.at[k - 1], (r, zk[k], t))
    loads[("up", 1)].wait()
    ups[1] = upf[1].astype(bf)
    loads[("up", 3)].wait()
    ups[3] = upf[3].astype(bf)
    up_send(1, None, early)
    up_send(1, inner, late)

    loads["tok"].wait()
    full = tok[...].astype(f32)
    inv = lax.rsqrt(jnp.mean(full * full, axis=-1, keepdims=True) + norm_eps)
    cols = pl.ds(mul(t, own), own)
    mine = tok[:, cols].astype(f32)
    normed = (mine * inv * mg[:, cols]).astype(bf)
    window = jnp.left_shift(jnp.int32(2), t)
    ti = lax.broadcasted_iota(jnp.int32, (LENGTH, LENGTH), 0)
    si = lax.broadcasted_iota(jnp.int32, (LENGTH, LENGTH), 1)
    band = jnp.where((ti - si >= 0) & (ti - si < window), 1.0, 0.0).astype(bf)
    pos = lax.broadcasted_iota(jnp.int32, (LENGTH, own), 0)
    divisor = jnp.minimum(pos + 1, window).astype(f32)
    for s in range(rows // LENGTH):
        part = normed[s * LENGTH:(s + 1) * LENGTH]
        summed = jnp.dot(band, part, preferred_element_type=f32)
        xn[0, s * LENGTH:(s + 1) * LENGTH, :own] = (summed / divisor - part.astype(f32)).astype(bf)

    def gw_swap(k):
        b = gw_at(zk[k], r)
        got(b, rw.at[k - 1])
        send(b, b, "gwy", ry.at[0], (peer_r, z, t))

    def up_swap(k, parts=whole):
        for i in parts:
            b = up_at(zk[k], r, i)
            got(b, rwu.at[k - 1, i])
            send(b, b, "upy", ryu.at[0], (peer_r, z, t))

    with jax.named_scope("gwswap"):
        for k in (1, 2, 3):
            gw_swap(k)
        up_send(2, outer, early)
        up_send(3, outer, early)
    with jax.named_scope("gwswapped"):
        got(gwg.at[pl.ds(0, (Z - 1) * hg)], ry.at[0])
    with jax.named_scope("mix"):
        mixed = jnp.dot(xn[0, :, :own], gwg[...], preferred_element_type=f32) * gs[...]
        car[z, t] = (tok[:, cols].astype(f32) + mixed).astype(bf)
    H = rows // LENGTH
    hr = LENGTH
    is_in = lax.rem(lax.div(z + 1, 2), 2)
    blocks = (z, is_in * zk[1] + (1 - is_in) * zk[3], is_in * zk[3] + (1 - is_in) * zk[1], zk[2])

    def half(h):
        return pl.ds(h * hr, hr)

    def to_x(src, h):
        b = car.at[src, t, half(h)]
        send(b, b, "carx", rcx.at[src, h], (r, z, xp))

    def to_core(src, h, q):
        b = car.at[src, q, half(h)]
        send(b, b, "carc", rcc.at[src], (r, z, cp))

    def to_z(src, h, dev, when=None):
        b = car.at[src, t, half(h)]
        send(b, b, "carz", rcz.at[src, h], (r, dev, t), when)

    for h in range(H):
        to_z(z, h, zk[3])
        to_z(z, h, mate)
        to_x(z, h)
        to_core(z, h, t)
    up_send(3, inner)
    up_send(2, inner)

    with jax.named_scope("casts"):
        for k in (2, 3, 1):
            loads[("dn", k)].wait()
            for c in range(C):
                dns[k, c] = dnf[k, :, c * cw:(c + 1) * cw].astype(bf)
        loads[("up", 0)].wait()
        upg[pl.ds(pl.multiple_of(z * 2 * hu + r * hu, hu), hu), :] = upf[0].astype(bf)
        loads["upo"].wait()
        upg[pl.ds(pl.multiple_of(z * 2 * hu + peer_r * hu, hu), hu), :] = upo[...].astype(bf)
        loads[("dn", 0)].wait()
        loads["dno"].wait()
        for c in range(C):
            here = pl.ds(mul(z, cw), cw)
            dng[c, pl.ds(mul(r, hd), hd), here] = dnf[0, :, c * cw:(c + 1) * cw].astype(bf)
            dng[c, pl.ds(mul(peer_r, hd), hd), here] = dno[:, c * cw:(c + 1) * cw].astype(bf)

    def arrive(d, h):
        src = blocks[d]
        got(car.at[src, t, half(h)], rcz.at[src, h])
        if d < 3:
            to_z(src, h, mate, outer if d == 1 else inner)
        to_x(src, h)
        to_core(src, h, t)

    def from_x(d, h):
        src = blocks[d]
        got(car.at[src, xp, half(h)], rcx.at[src, h])
        to_core(src, h, xp)

    def dn_group(*pieces):
        for c, k in pieces:
            dn_send(c, k)

    def dn_outer(c):
        dn_group((c, 3), (c, 2), (c, 1))

    def dn_forward(c, k):
        src = zk[k]
        got(dn_at(c, src, r), rwd.at[k - 1, c])
        send(dn_at(c, src, r), dn_at(c, src, r), "dny", ryd.at[c], (peer_r, z, t))

    def norm(d):
        src = blocks[d]
        got(car.at[src, pl.ds(0, 2)], rcc.at[src])
        total = jnp.zeros((rows, 1), f32)
        for q in range(T):
            c = car[src, q].astype(f32)
            total += jnp.sum(c * c, axis=-1, keepdims=True)
        scale = lax.rsqrt(total / D + norm_eps)
        for q in range(T):
            part = slice(q * own, (q + 1) * own)
            xn[d, :, part] = (car[src, q].astype(f32) * scale * lg[:, part]).astype(bf)

    def up(d):
        pre = jnp.dot(xn[d], upg[...], preferred_element_type=f32)
        pre = jnp.maximum(pre * us[:, pl.ds(mul(z, fsub), fsub)], 0.0)
        hid[blocks[d]] = (pre * pre).astype(bf)

    def dn_ready(c):
        got(dns.at[0, pl.ds(0, Z - 1)], ryd.at[c])

    def down(c, k):
        src = zk[k]
        p = jnp.dot(hid[src], dng[c], preferred_element_type=f32)
        for q in range(T):
            part = p[:, q * cw:(q + 1) * cw] * ds[:, q * own + c * cw:q * own + (c + 1) * cw]
            pb[c, src, q] = part.astype(bf)
        for j, q in ((1, cxp), (0, cp)):
            send(pb.at[c, src, q], ra.at[c, src, j], "pb", rx.at[c, src] if j else rj.at[c], (r, z, cp))

    def over_x(c, k):
        src = zk[k]
        got(ra.at[c, src, 1], rx.at[c, src])
        sx[c, src] = (pb[c, src, xp].astype(f32) + ra[c, src, 1].astype(f32)).astype(bf)
        send(sx.at[c, src], rb.at[c, src], "sx", rb_s.at[c, src], (r, z, xp))

    def both(c, src):
        return pb[c, src, t].astype(f32) + ra[c, src, 0].astype(f32) + rb[c, src].astype(f32)

    def joined(c, k):
        src = zk[k]
        if k == 2:
            got(sx.at[c], rj.at[c])
        got(rb.at[c, src], rb_s.at[c, src])

    def to_side(c):
        src = zk[2]
        joined(c, 2)
        sz[c, src] = both(c, src).astype(bf)
        send(sz.at[c, src], ri.at[c], "sz", rm.at[c], (r, mate, t))

    def across(c):
        src = zk[3]
        joined(c, 3)
        got(ri.at[c], rm.at[c])
        sz[c, src] = (both(c, src) + ri[c].astype(f32)).astype(bf)
        send(sz.at[c, src], rc.at[c, 1], "sz", rt.at[c, 1], (r, src, t))

    def to_mate(c):
        joined(c, 1)
        sz[c, mate] = both(c, mate).astype(bf)
        send(sz.at[c, mate], rc.at[c, 0], "sz", rt.at[c, 0], (r, mate, t))

    def write(c, q):
        pltpu.make_async_copy(
            og.at[c, q], out_h.at[:, pl.ds(pl.multiple_of(q * own + c * cw, cw), cw)], sent.at[len(groups)]
        ).start()

    def pass_on(c, q, rs, dev):
        send(og.at[c, q], og.at[c, q], "og", rs, dev)

    def finish(c):
        joined(c, 0)
        acc = both(c, z) + car[z, t, :, :].astype(f32)[:, c * cw:(c + 1) * cw]
        for j in range(2):
            got(rc.at[c, j], rt.at[c, j])
            acc += rc[c, j].astype(f32)
        og[c, t] = acc.astype(bf)
        pass_on(c, t, ro.at[c], (r, z, xp))
        pass_on(c, t, rq.at[c], (r, z, cp))
        write(c, t)

    def spread(c):
        got(og.at[c, xp], ro.at[c])
        pass_on(c, xp, rq.at[c], (r, z, cp))
        write(c, xp)

    def collect(c):
        got(og.at[c, pl.ds(0, 2)], rq.at[c])
        write(c, cp)
        write(c, cxp)

    def up_ready():
        got(ups.at[pl.ds(0, Z - 1)], ryu.at[0])

    def forward(c):
        for k in (1, 2, 3):
            run("fwd", dn_forward, c, k)

    def halves(name, fn, d):
        for h in range(H):
            run(name, fn, d, h)

    only(outer, ("ous3", up_swap, 3, early))
    only(inner, ("ius1", up_swap, 1, early), ("ius2", up_swap, 2, early))
    halves("fx", from_x, 0)
    halves("arr", arrive, 1)
    only(
        outer, ("ou2", up_send, 2, None, late), ("ou3", up_send, 3, None, late), ("ou1", up_send, 1, None, late),
        ("ous1", up_swap, 1), ("ofx", from_x, 1, 0), ("ofx", from_x, 1, 1),
    )
    halves("arr", arrive, 2)
    only(
        inner, ("ifx", from_x, 1, 0), ("ifx", from_x, 1, 1), ("iarr", arrive, 3, 0), ("iarr", arrive, 3, 1),
        ("dn", dn_outer, 0), ("dn", dn_outer, 1),
        ("ius2", up_swap, 2, late), ("ius3", up_swap, 3),
        ("ifx", from_x, 2, 0), ("ifx", from_x, 2, 1),
        ("ius1", up_swap, 1, late), ("dn", dn_outer, 2), ("dn", dn_outer, 3),
    )
    only(
        outer, ("ofx", from_x, 2, 0), ("ofx", from_x, 2, 1), ("oarr", arrive, 3, 0), ("oarr", arrive, 3, 1),
        ("dn", dn_outer, 0), ("dn", dn_outer, 1), ("ous3", up_swap, 3, late), ("ous2", up_swap, 2),
    )
    halves("fx", from_x, 3)
    for d in range(Z):
        run("norm", norm, d)
    run("usd", up_ready)
    forward(0)
    only(outer, ("dn", dn_outer, 2))
    for d in range(Z):
        run("up", up, d)
    forward(1)
    only(outer, ("dn", dn_outer, 3))
    for c in range(C):
        run("ready", dn_ready, c)
        for k in (2, 3, 1, 0):
            run("down", down, c, k)
        if c > 0:
            run("side", to_side, c - 1)
        for k in (2, 3, 1, 0):
            run("x", over_x, c, k)
        if c + 2 < C:
            forward(c + 2)
        if c > 0:
            run("mate", to_mate, c - 1)
            run("across", across, c - 1)
        if c > 1:
            run("fin", finish, c - 2)
    run("side", to_side, C - 1)
    run("mate", to_mate, C - 1)
    run("across", across, C - 1)
    run("fin", finish, C - 2)
    for c in range(C - 2):
        run("spread", spread, c)
    for c in range(C - 2):
        run("coll", collect, c)
    run("spread", spread, C - 2)
    run("fin", finish, C - 1)
    run("coll", collect, C - 2)
    run("spread", spread, C - 1)
    run("coll", collect, C - 1)
    with jax.named_scope("drain"):
        drain()


def fused(mesh_shape, tokens, mix_gain, group_weight, group_scale, mlp_gain, up_weight, up_scale, down_weight, down_scale):
    Z, T = mesh_shape["fs"], mesh_shape["tp"]
    C = CHUNKS
    rows, D = tokens.shape
    own = group_weight.shape[1]
    hg, hu = group_weight.shape[0] // 2, up_weight.shape[0] // 2
    fsub = up_weight.shape[1] // Z
    hd = fsub // 2
    dsub = down_weight.shape[1]
    cw = dsub // C
    bf, f32 = jnp.bfloat16, jnp.float32
    dma = pltpu.SemaphoreType.DMA
    vm = pl.BlockSpec(memory_space=pltpu.VMEM)
    hbm = pl.BlockSpec(memory_space=pl.ANY)
    sizes = (Z, T, C, rows, D, own, hg, hu, hd, fsub, dsub)
    V = pltpu.VMEM
    H = rows // LENGTH
    piece = (C, Z, rows, cw)
    return pl.pallas_call(
        functools.partial(ring_kernel, sizes),
        out_shape=jax.ShapeDtypeStruct((rows, D), bf),
        in_specs=[hbm, vm, hbm, vm, vm, hbm, vm, hbm, vm],
        out_specs=hbm,
        scratch_shapes=[
            V((rows, D), bf), V((2 * hg, own), f32),
            V((Z, hu, fsub), f32), V((hu, fsub), f32), V((Z, hd, dsub), f32), V((hd, dsub), f32),
            V((Z * 2 * hg, own), bf), V((Z, hu, fsub), bf), V((Z * 2 * hu, fsub), bf),
            V((Z, C, hd, cw), bf), V((C, 2 * hd, Z * cw), bf),
            V((Z, T, rows, own), bf), V((Z, rows, D), bf), V((Z, rows, fsub), bf), V((C, Z, T, rows, cw), bf),
            V((C, Z, 2, rows, cw), bf), V(piece, bf), V(piece, bf), V(piece, bf), V((C, rows, cw), bf),
            V((C, 2, rows, cw), bf), V((C, T, rows, cw), bf),
            dma((4 + 2 * Z,)), dma((14,)), dma((3,)), dma((1,)), dma((3, PARTS)), dma((1,)), dma((3, C)), dma((C,)),
            dma((Z, H)), dma((Z, H)), dma((Z,)), dma((C, Z)), dma((C,)), dma((C, Z)), dma((C, 2)), dma((C,)),
            dma((C,)), dma((C,)),
        ],
        compiler_params=pltpu.CompilerParams(
            collective_id=0, has_side_effects=True, vmem_limit_bytes=60 * 1024 * 1024
        ),
    )(
        tokens, mix_gain[None], group_weight, group_scale, mlp_gain[None],
        up_weight, up_scale, down_weight, down_scale,
    )


def fits(mesh):
    shape = mesh.shape
    return shape["rep"] == 2 and shape["tp"] == GROUPS and shape["fs"] == shape["tp"]


def solution(mesh):
    in_specs = (
        P(("rep", "fs"), None),
        P(),
        P("fs", "tp"),
        P(None, "tp"),
        P(),
        P("fs", "tp"),
        P(None, "tp"),
        P("tp", "fs"),
        P(),
    )
    out_specs = P(("rep", "fs"), None)
    chosen = functools.partial(fused, mesh.shape) if fits(mesh) else body
    return jax.shard_map(chosen, mesh=mesh, in_specs=in_specs, out_specs=out_specs, check_vma=False)
```

time: 116 us -> 104 us (0.90)
  Pallas kernels: 113 us -> 101 us
    pallas_call x1, Pallas kernels: 113 us -> 101 us  [fused(): pl.pallas_call(functools.partial(ring_kernel, sizes), out_shape=jax.Shape...]
where the time goes in v2:
time: 104 us
  Pallas kernels  101 us (97%)
  local copies, waits for them, and re-layouts  2.3 us (2%)
    pallas_call x1, Pallas kernels, fused(): pl.pallas_call(functools.partial(ring_kernel, sizes), out_shape=jax.Shape...  101 us
    unnamed x1, local copies, waits for them, and re-layouts  2.3 us

profile of v2, /device:TPU:1, one launch (start us, length us, event | category | flops | bytes accessed | tf_op | source)
XLA Modules:
  0.0 103.5 jit_solution(12176957102175731961)
XLA Ops:
  0.0 101.2 %shard_map.91 = bf16[256,2048]{1,0:T(8,128)(2,1)} custom-call(bf16[256,2048]{1,0:T(8,128)(2,1)} %tok_h.1, f32[1,2048]{1,0:T(1,128)} %bitcast.2, f32[128,512]{1,0:T(8,128)} %gw_h.1, f32[1,512]{1,0:T(1,128)} %gs.1, f32[1,2048]{1,0:T(1,128)} %bitcast.3, f32[512,2048]{1,0:T(8,128)} %up_h.1, f32[1,2048]{1,0:T(1,128)} %us.1, f32[2048,512]{1,0:T(8,128)} %dn_h.1, ...), custom_call_target="tpu_custom_call" | custom-call | tf_op jit(solution)/shard_map/pallas_call | solution.py:520
  101.2 2.3 %copy.11 = bf16[256,2048]{1,0:T(8,128)(2,1)} copy(bf16[256,2048]{1,0:T(8,128)(2,1)} %shard_map.91) | data formatting | bytes 2097152

commit v3 on v2

--- a/solution.py
+++ b/solution.py
@@ -93,11 +93,12 @@
 
 def ring_kernel(
     sizes,
-    tok_h, mg, gw_h, gs, lg, up_h, us, dn_h, ds,
+    tok_h, mg_h, gw_h, gs_h, lg_h, up_h, us_h, dn_h, ds_h,
     out_h,
+    mg, gs, lg, us, ds,
     tok, gwf, upf, upo, dnf, dno,
     gwg, ups, upg, dns, dng,
-    car, xn, hid, pb, ra, sx, rb, sz, ri, rc, og,
+    car, xn, hid, pb, ra, sx, rb, sz, ri, rc,
     ld, sent, rw, ry, rwu, ryu, rwd, ryd, rcz, rcx, rcc, rx, rj, rb_s, rt, rm, ro, rq,
 ):
     Z, T, C, rows, D, own, hg, hu, hd, fsub, dsub = sizes
@@ -138,6 +139,9 @@
     load("upo", up_h.at[pl.ds(mul(peer_r, hu), hu), pl.ds(mul(z, fsub), fsub)], upo, 2 + 2 * Z)
     for k in (2, 3, 1, 0):
         load_dn(k)
+    small = (("mg", mg_h, mg), ("gs", gs_h, gs), ("lg", lg_h, lg), ("us", us_h, us), ("ds", ds_h, ds))
+    for i, (key, src, dst) in enumerate(small):
+        load(key, src, dst, 4 + 2 * Z + i)
     load("dno", dn_h.at[pl.ds(pl.multiple_of(z * 2 * hd + peer_r * hd, hd), hd), :], dno, 3 + 2 * Z)
 
     barrier = pltpu.get_barrier_semaphore()
@@ -178,11 +182,10 @@
         same = (
             gwg.at[pl.ds(0, (Z - 1) * hg)], gwg.at[pl.ds(0, (Z - 1) * hg)], ups.at[three], ups.at[three],
             dns.at[three], dns.at[three], car.at[0, three], car.at[0], car.at[pl.ds(0, 2)],
-            ra, rb, og.at[:, three], og.at[:, three],
+            ra, rb, sx.at[:, three], sx.at[:, three],
         )
         for i, ref in enumerate(same):
             remote(ref, ref, sent.at[i], rcc.at[0], (peer_r, z, t)).wait_send()
-        pltpu.make_async_copy(out_h, out_h, sent.at[len(same)]).wait()
 
     def got(dst, rs):
         guarded(lambda: remote(dst, dst, sent.at[0], rs, (peer_r, z, t)).wait_recv())
@@ -228,7 +231,8 @@
     up_send(1, None, early)
     up_send(1, inner, late)
 
-    loads["tok"].wait()
+    for key in ("tok", "mg", "gs", "lg", "us", "ds"):
+        loads[key].wait()
     full = tok[...].astype(f32)
     inv = lax.rsqrt(jnp.mean(full * full, axis=-1, keepdims=True) + norm_eps)
     cols = pl.ds(mul(t, own), own)
@@ -291,8 +295,8 @@
         to_z(z, h, mate)
         to_x(z, h)
         to_core(z, h, t)
+    up_send(2, inner)
     up_send(3, inner)
-    up_send(2, inner)
 
     with jax.named_scope("casts"):
         for k in (2, 3, 1):
@@ -397,13 +401,11 @@
         sz[c, mate] = both(c, mate).astype(bf)
         send(sz.at[c, mate], rc.at[c, 0], "sz", rt.at[c, 0], (r, mate, t))
 
-    def write(c, q):
-        pltpu.make_async_copy(
-            og.at[c, q], out_h.at[:, pl.ds(pl.multiple_of(q * own + c * cw, cw), cw)], sent.at[len(groups)]
-        ).start()
+    def og(c, q):
+        return out_h.at[:, pl.ds(pl.multiple_of(q * own + c * cw, cw), cw)]
 
     def pass_on(c, q, rs, dev):
-        send(og.at[c, q], og.at[c, q], "og", rs, dev)
+        send(og(c, q), og(c, q), "og", rs, dev)
 
     def finish(c):
         joined(c, 0)
@@ -411,20 +413,16 @@
         for j in range(2):
             got(rc.at[c, j], rt.at[c, j])
             acc += rc[c, j].astype(f32)
-        og[c, t] = acc.astype(bf)
+        out_h[:, pl.ds(pl.multiple_of(t * own + c * cw, cw), cw)] = acc.astype(bf)
         pass_on(c, t, ro.at[c], (r, z, xp))
         pass_on(c, t, rq.at[c], (r, z, cp))
-        write(c, t)
 
     def spread(c):
-        got(og.at[c, xp], ro.at[c])
+        got(og(c, xp), ro.at[c])
         pass_on(c, xp, rq.at[c], (r, z, cp))
-        write(c, xp)
 
     def collect(c):
-        got(og.at[c, pl.ds(0, 2)], rq.at[c])
-        write(c, cp)
-        write(c, cxp)
+        got(sx.at[c, pl.ds(0, 2)], rq.at[c])
 
     def up_ready():
         got(ups.at[pl.ds(0, Z - 1)], ryu.at[0])
@@ -455,12 +453,13 @@
     )
     only(
         outer, ("ofx", from_x, 2, 0), ("ofx", from_x, 2, 1), ("oarr", arrive, 3, 0), ("oarr", arrive, 3, 1),
-        ("dn", dn_outer, 0), ("dn", dn_outer, 1), ("ous3", up_swap, 3, late), ("ous2", up_swap, 2),
+        ("ous3", up_swap, 3, late), ("ous2", up_swap, 2), ("dn", dn_outer, 0),
     )
     halves("fx", from_x, 3)
     for d in range(Z):
         run("norm", norm, d)
     run("usd", up_ready)
+    only(outer, ("dn", dn_outer, 1))
     forward(0)
     only(outer, ("dn", dn_outer, 2))
     for d in range(Z):
@@ -512,34 +511,38 @@
     bf, f32 = jnp.bfloat16, jnp.float32
     dma = pltpu.SemaphoreType.DMA
     vm = pl.BlockSpec(memory_space=pltpu.VMEM)
-    hbm = pl.BlockSpec(memory_space=pl.ANY)
+    hbm = pl.BlockSpec(memory_space=pltpu.HBM)
     sizes = (Z, T, C, rows, D, own, hg, hu, hd, fsub, dsub)
     V = pltpu.VMEM
     H = rows // LENGTH
     piece = (C, Z, rows, cw)
+    pin = functools.partial(pltpu.with_memory_space_constraint, memory_space=pltpu.HBM)
     return pl.pallas_call(
         functools.partial(ring_kernel, sizes),
         out_shape=jax.ShapeDtypeStruct((rows, D), bf),
-        in_specs=[hbm, vm, hbm, vm, vm, hbm, vm, hbm, vm],
-        out_specs=hbm,
+        in_specs=[hbm] * 9,
+        out_specs=vm,
         scratch_shapes=[
+            V((1, D), f32), V((1, own), f32), V((1, D), f32), V((1, Z * fsub), f32), V((1, D), f32),
             V((rows, D), bf), V((2 * hg, own), f32),
             V((Z, hu, fsub), f32), V((hu, fsub), f32), V((Z, hd, dsub), f32), V((hd, dsub), f32),
             V((Z * 2 * hg, own), bf), V((Z, hu, fsub), bf), V((Z * 2 * hu, fsub), bf),
             V((Z, C, hd, cw), bf), V((C, 2 * hd, Z * cw), bf),
             V((Z, T, rows, own), bf), V((Z, rows, D), bf), V((Z, rows, fsub), bf), V((C, Z, T, rows, cw), bf),
             V((C, Z, 2, rows, cw), bf), V(piece, bf), V(piece, bf), V(piece, bf), V((C, rows, cw), bf),
-            V((C, 2, rows, cw), bf), V((C, T, rows, cw), bf),
-            dma((4 + 2 * Z,)), dma((14,)), dma((3,)), dma((1,)), dma((3, PARTS)), dma((1,)), dma((3, C)), dma((C,)),
+            V((C, 2, rows, cw), bf),
+            dma((9 + 2 * Z,)), dma((13,)), dma((3,)), dma((1,)), dma((3, PARTS)), dma((1,)), dma((3, C)), dma((C,)),
             dma((Z, H)), dma((Z, H)), dma((Z,)), dma((C, Z)), dma((C,)), dma((C, Z)), dma((C, 2)), dma((C,)),
             dma((C,)), dma((C,)),
         ],
         compiler_params=pltpu.CompilerParams(
-            collective_id=0, has_side_effects=True, vmem_limit_bytes=60 * 1024 * 1024
+            collective_id=0, has_side_effects=True, vmem_limit_bytes=48000 * 1024
         ),
     )(
-        tokens, mix_gain[None], group_weight, group_scale, mlp_gain[None],
-        up_weight, up_scale, down_weight, down_scale,
+        *(pin(a) for a in (
+            tokens, mix_gain[None], group_weight, group_scale, mlp_gain[None],
+            up_weight, up_scale, down_weight, down_scale,
+        ))
     )
 
 

time: 104 us -> 100 us (0.962)
  Pallas kernels: 101 us -> 99.2 us
  local copies, waits for them, and re-layouts: 2.3 us -> 0.97 us
    pallas_call x1, Pallas kernels: 101 us -> 99.2 us  [fused(): pl.pallas_call(functools.partial(ring_kernel, sizes), out_shape=jax.Shape...]
    unnamed x1, local copies, waits for them, and re-layouts: 2.3 us -> 0.97 us
where the time goes in v3:
time: 100 us
  Pallas kernels  99.2 us (99%)
    pallas_call x1, Pallas kernels, fused(): pl.pallas_call(functools.partial(ring_kernel, sizes), out_shape=jax.Shape...  99.2 us

profile of v3, /device:TPU:1, one launch (start us, length us, event | category | flops | bytes accessed | tf_op | source)
XLA Modules:
  0.0 100.1 jit_solution(15873526486817137545)
XLA Ops:
  0.0 99.2 %shard_map.91 = bf16[256,2048]{1,0:T(8,128)(2,1)S(1)} custom-call(bf16[256,2048]{1,0:T(8,128)(2,1)} %tok_h.1, f32[1,2048]{1,0:T(1,128)} %bitcast.2, f32[128,512]{1,0:T(8,128)} %gw_h.1, f32[1,512]{1,0:T(1,128)} %gs_h.1, f32[1,2048]{1,0:T(1,128)} %bitcast.3, f32[512,2048]{1,0:T(8,128)} %up_h.1, f32[1,2048]{1,0:T(1,128)} %us_h.1, f32[2048,512]{1,0:T(8,128)} %dn_h.1, ...), custom_call_target="tpu_custom_call" | custom-call | tf_op jit(solution)/shard_map/pallas_call | solution.py:520
  99.2 1.0 copy.11

commit v4 on v3

--- a/solution.py
+++ b/solution.py
@@ -260,6 +260,7 @@
             got(b, rwu.at[k - 1, i])
             send(b, b, "upy", ryu.at[0], (peer_r, z, t))
 
+    up_send(2, inner, early)
     with jax.named_scope("gwswap"):
         for k in (1, 2, 3):
             gw_swap(k)
@@ -295,8 +296,10 @@
         to_z(z, h, mate)
         to_x(z, h)
         to_core(z, h, t)
-    up_send(2, inner)
-    up_send(3, inner)
+    up_send(3, inner, early)
+    for parts in (late,):
+        up_send(2, inner, parts)
+        up_send(3, inner, parts)
 
     with jax.named_scope("casts"):
         for k in (2, 3, 1):
@@ -447,20 +450,21 @@
     only(
         inner, ("ifx", from_x, 1, 0), ("ifx", from_x, 1, 1), ("iarr", arrive, 3, 0), ("iarr", arrive, 3, 1),
         ("dn", dn_outer, 0), ("dn", dn_outer, 1),
-        ("ius2", up_swap, 2, late), ("ius3", up_swap, 3),
+        ("ius2", up_swap, 2, late), ("ius1", up_swap, 1, late),
         ("ifx", from_x, 2, 0), ("ifx", from_x, 2, 1),
-        ("ius1", up_swap, 1, late), ("dn", dn_outer, 2), ("dn", dn_outer, 3),
+        ("ius3", up_swap, 3), ("dn", dn_outer, 2), ("dn", dn_outer, 3),
     )
     only(
-        outer, ("ofx", from_x, 2, 0), ("ofx", from_x, 2, 1), ("oarr", arrive, 3, 0), ("oarr", arrive, 3, 1),
-        ("ous3", up_swap, 3, late), ("ous2", up_swap, 2), ("dn", dn_outer, 0),
+        outer, ("ous3", up_swap, 3, late), ("ofx", from_x, 2, 0), ("ofx", from_x, 2, 1),
+        ("ous2", up_swap, 2, early), ("oarr", arrive, 3, 0), ("oarr", arrive, 3, 1),
+        ("ous2", up_swap, 2, late), ("dn", dn_outer, 0),
     )
     halves("fx", from_x, 3)
     for d in range(Z):
         run("norm", norm, d)
+    forward(0)
+    only(outer, ("dn", dn_outer, 1))
     run("usd", up_ready)
-    only(outer, ("dn", dn_outer, 1))
-    forward(0)
     only(outer, ("dn", dn_outer, 2))
     for d in range(Z):
         run("up", up, d)
@@ -472,28 +476,35 @@
             run("down", down, c, k)
         if c > 0:
             run("side", to_side, c - 1)
-        for k in (2, 3, 1, 0):
+        for k in (2, 3):
             run("x", over_x, c, k)
+        for i in range(C - 2 if c == C - 1 else c, c + 1):
+            if c != C - 2:
+                for k in (1, 0):
+                    run("x", over_x, i, k)
         if c + 2 < C:
             forward(c + 2)
         if c > 0:
-            run("mate", to_mate, c - 1)
+            if c < C - 1:
+                run("mate", to_mate, c - 1)
             run("across", across, c - 1)
-        if c > 1:
-            run("fin", finish, c - 2)
     run("side", to_side, C - 1)
+    run("fin", finish, 0)
+    run("mate", to_mate, C - 2)
+    for c in range(1, C - 2):
+        run("fin", finish, c)
+    run("across", across, C - 1)
     run("mate", to_mate, C - 1)
-    run("across", across, C - 1)
     run("fin", finish, C - 2)
     for c in range(C - 2):
         run("spread", spread, c)
+    run("fin", finish, C - 1)
     for c in range(C - 2):
         run("coll", collect, c)
-    run("spread", spread, C - 2)
-    run("fin", finish, C - 1)
-    run("coll", collect, C - 2)
-    run("spread", spread, C - 1)
-    run("coll", collect, C - 1)
+    for c in (C - 2, C - 1):
+        run("spread", spread, c)
+    for c in (C - 2, C - 1):
+        run("coll", collect, c)
     with jax.named_scope("drain"):
         drain()
 

time: 100 us -> 95.7 us (0.957)
  Pallas kernels: 99.2 us -> 94.5 us
    pallas_call x1, Pallas kernels: 99.2 us -> 94.5 us  [fused(): pl.pallas_call(functools.partial(ring_kernel, sizes), out_shape=jax.Shape...]
where the time goes in v4:
time: 95.7 us; the launch traced here: 95.4 us
  Pallas kernels  94.5 us (99%)
  local copies, waits for them, and re-layouts  0.97 us (1%)
    pallas_call x1, Pallas kernels, fused(): pl.pallas_call(functools.partial(ring_kernel, sizes), out_shape=jax.Shape...  94.5 us

profile of v4, /device:TPU:1, one launch (start us, length us, event | category | flops | bytes accessed | tf_op | source)
XLA Modules:
  0.0 95.4 jit_solution(17684959947426027785)
XLA Ops:
  0.0 94.5 %shard_map.91 = bf16[256,2048]{1,0:T(8,128)(2,1)S(1)} custom-call(bf16[256,2048]{1,0:T(8,128)(2,1)} %tok_h.1, f32[1,2048]{1,0:T(1,128)} %bitcast.2, f32[128,512]{1,0:T(8,128)} %gw_h.1, f32[1,512]{1,0:T(1,128)} %gs_h.1, f32[1,2048]{1,0:T(1,128)} %bitcast.3, f32[512,2048]{1,0:T(8,128)} %up_h.1, f32[1,2048]{1,0:T(1,128)} %us_h.1, f32[2048,512]{1,0:T(8,128)} %dn_h.1, ...), custom_call_target="tpu_custom_call" | custom-call | tf_op jit(solution)/shard_map/pallas_call | solution.py:531
  94.5 1.0 %copy.11 = bf16[256,2048]{1,0:T(8,128)(2,1)} copy(bf16[256,2048]{1,0:T(8,128)(2,1)S(1)} %shard_map.91) | data formatting | bytes 2097152

commit v5 on v4

--- a/solution.py
+++ b/solution.py
@@ -264,8 +264,8 @@
     with jax.named_scope("gwswap"):
         for k in (1, 2, 3):
             gw_swap(k)
+        up_send(3, outer, early)
         up_send(2, outer, early)
-        up_send(3, outer, early)
     with jax.named_scope("gwswapped"):
         got(gwg.at[pl.ds(0, (Z - 1) * hg)], ry.at[0])
     with jax.named_scope("mix"):

time: 95.7 us -> 95.7 us (level)
  no operation moved by 1% of the time
where the time goes in v5:
time: 95.7 us; the launch traced here: 95.4 us
  Pallas kernels  94.5 us (99%)
  local copies, waits for them, and re-layouts  0.97 us (1%)
    pallas_call x1, Pallas kernels, fused(): pl.pallas_call(functools.partial(ring_kernel, sizes), out_shape=jax.Shape...  94.5 us

profile of v5, /device:TPU:1, one launch (start us, length us, event | category | flops | bytes accessed | tf_op | source)
XLA Modules:
  0.0 95.4 jit_solution(2850363304598055882)
XLA Ops:
  0.0 94.5 %shard_map.91 = bf16[256,2048]{1,0:T(8,128)(2,1)S(1)} custom-call(bf16[256,2048]{1,0:T(8,128)(2,1)} %tok_h.1, f32[1,2048]{1,0:T(1,128)} %bitcast.2, f32[128,512]{1,0:T(8,128)} %gw_h.1, f32[1,512]{1,0:T(1,128)} %gs_h.1, f32[1,2048]{1,0:T(1,128)} %bitcast.3, f32[512,2048]{1,0:T(8,128)} %up_h.1, f32[1,2048]{1,0:T(1,128)} %us_h.1, f32[2048,512]{1,0:T(8,128)} %dn_h.1, ...), custom_call_target="tpu_custom_call" | custom-call | tf_op jit(solution)/shard_map/pallas_call | solution.py:531
  94.5 1.0 %copy.11 = bf16[256,2048]{1,0:T(8,128)(2,1)} copy(bf16[256,2048]{1,0:T(8,128)(2,1)S(1)} %shard_map.91) | data formatting | bytes 2097152
